TPU v7x, 256 devices: a whole 4x4x8 slice. The times are simulated.
256 devices in a mesh: sp: 64 (over z, y, core), tp: 4 (over x).
Axes of the slice: x: 4, y: 4, z: 8, core: 2. Of those that a mesh axis runs over, the one named last changes fastest.
Arguments:
- stream_in: bfloat16 [16384, 2048], P(('sp', 'tp')), may hold values from -6 to 6
- queries_one: bfloat16 [16384, 1024], P('sp', 'tp'), may hold values from -120 to 120
- queries_two: bfloat16 [16384, 1024], P('sp', 'tp'), may hold values from -120 to 120
- keys_one: bfloat16 [16384, 512], P('sp', 'tp'), may hold values from -7 to 7
- keys_two: bfloat16 [16384, 512], P('sp', 'tp'), may hold values from -7 to 7
- values: bfloat16 [16384, 1024], P('sp', 'tp'), may hold values from -6 to 6
- lambdas: float32 [8], P('tp'), may hold values from 0.3 to 0.8
- head_gain: float32 [256], replicated, may hold values from 0.1 to 1.9
- out_weight: bfloat16 [2048, 2048], P('tp'), may hold values from -0.125 to 0.125
- norm_gain: float32 [2048], replicated, may hold values from 0.1 to 1.9
- expert_ids: int32 [16384, 2], P(('sp', 'tp')), may hold values from 0 to 63, all different within a row; in each aligned block of 64 rows (0 to 63, 64 to 127, ...) at most 4 rows name the same one
- route_weight: float32 [16384, 2], P(('sp', 'tp')), may hold values from 0.1 to 1
- gate_weight: bfloat16 [64, 2048, 1024], P('sp', None, 'tp'), may hold values from -0.125 to 0.125
- up_weight: bfloat16 [64, 2048, 1024], P('sp', None, 'tp'), may hold values from -0.125 to 0.125
- down_weight: bfloat16 [64, 1024, 2048], P('sp', 'tp'), may hold values from -0.1875 to 0.1875
Outputs:
- mixed: bfloat16 [16384, 2048], P(('sp', 'tp'))
Inputs may be any that keep to these rules, and one draw needn't show every extreme that they name: `expert_ids`: each row names 2 different experts. In each aligned block of 64 rows no expert is named more than 4 times, a bound that some block reaches.
All inputs are finite; a program needn't handle non-finite values.
Results may differ from a plain program's by a relative error of at most 0.013.
Values may be sent and summed in bfloat16 or wider, within the bound.
No kernel may reach another device: no remote copies, remote signals or barrier semaphores. Data moves between devices by JAX's collectives and lax.ppermute only.
A program may use at most 128 MiB of HBM per device.

v0:
```python
import math

import jax
import jax.numpy as jnp
from jax import lax
from jax.sharding import PartitionSpec as P

HEAD_DIM = 128
VAL_DIM = 256


EPS = 1e-06
OUT_SCALE = 0.8


def cut_along(x, dim, peers):
    before, after = (x.shape[:dim], x.shape[dim + 1 :])
    return jnp.moveaxis(x.reshape(*before, peers, -1, *after), dim, 0)


def sum_at_owner(x, axis, dim):
    peers = lax.axis_size(axis)
    tiles = lax.all_to_all(cut_along(x, dim, peers), axis, 0, 0, tiled=True)
    return jnp.sum(tiles.astype(jnp.float32), axis=0)


def update_map(carried, queries, keys, vals, allowed):
    row_max, totals, accum = carried
    scores = jnp.einsum(
        "qgrd,kgd->grqk", queries, keys, preferred_element_type=jnp.float32
    ) * HEAD_DIM ** (-0.5)
    scores = jnp.where(allowed[None, None], scores, -jnp.inf)
    new_max = jnp.maximum(row_max, jnp.max(scores, axis=-1))
    safe_max = jnp.where(new_max == -jnp.inf, 0.0, new_max)
    exp_terms = jnp.exp(scores - safe_max[..., None])
    rescale = jnp.exp(row_max - safe_max)
    totals = totals * rescale + jnp.sum(exp_terms, axis=-1)
    accum = accum * rescale[..., None] + jnp.einsum(
        "grqk,kgv->grqv", exp_terms.astype(jnp.bfloat16), vals, preferred_element_type=jnp.float32
    )
    return (new_max, totals, accum)


def fold_piece(carried, piece, q_first, q_second, query_pos, shape_info):
    kv_here, head_dim, val_dim = shape_info
    piece_rows = piece.shape[0]
    key_block = math.gcd(piece_rows, 1024)
    num_blocks = piece_rows // key_block
    last_query = jnp.max(query_pos)

    def advance(block_no, carry_now):
        first_key = block_no * key_block

        def compute(carry_in):
            rows_now = lax.dynamic_slice_in_dim(piece, block_no * key_block, key_block, 0)
            key_first = rows_now[:, : kv_here * head_dim].reshape(key_block, kv_here, head_dim)
            key_second = rows_now[:, kv_here * head_dim : 2 * kv_here * head_dim].reshape(
                key_block, kv_here, head_dim
            )
            vals = rows_now[:, 2 * kv_here * head_dim :].reshape(key_block, kv_here, val_dim)
            key_pos = first_key + lax.iota(jnp.int32, key_block)
            allowed = (key_pos[None, :] <= query_pos[:, None]) & (key_pos[None, :] >= 0)
            first_map = update_map(carry_in[0:3], q_first, key_first, vals, allowed)
            second_map = update_map(carry_in[3:6], q_second, key_second, vals, allowed)
            return first_map + second_map

        def unchanged(carry_in):
            return carry_in

        return lax.cond(first_key > last_query, unchanged, compute, carry_now)

    return lax.fori_loop(0, num_blocks, advance, carried)


def shards(
    stream_in,
    queries_one,
    queries_two,
    keys_one,
    keys_two,
    values,
    lambdas,
    head_gain,
    out_weight,
    norm_gain,
    expert_ids,
    route_weight,
    gate_weight,
    up_weight,
    down_weight,
):
    rows_q = queries_one.shape[0]
    heads_here = queries_one.shape[1] // HEAD_DIM
    kv_here = keys_one.shape[1] // HEAD_DIM
    per_kv = heads_here // kv_here
    position = lax.axis_index("sp")
    query_pos = position * rows_q + lax.iota(jnp.int32, rows_q)
    q_first = queries_one.reshape(rows_q, kv_here, per_kv, HEAD_DIM)
    q_second = queries_two.reshape(rows_q, kv_here, per_kv, HEAD_DIM)
    packed = jnp.concatenate([keys_one, keys_two, values], 1)
    shape_info = (kv_here, HEAD_DIM, VAL_DIM)
    max_init = jnp.full((kv_here, per_kv, rows_q), -jnp.inf, jnp.float32)
    sum_init = jnp.zeros((kv_here, per_kv, rows_q), jnp.float32)
    acc_init = jnp.zeros((kv_here, per_kv, rows_q, VAL_DIM), jnp.float32)
    initial = (max_init, sum_init, acc_init, max_init, sum_init, acc_init)
    final = fold_piece(
        initial,
        lax.all_gather(packed, "sp", axis=0, tiled=True),
        q_first,
        q_second,
        query_pos,
        shape_info,
    )
    mix_first = final[2] / final[1][..., None]
    mix_second = final[5] / final[4][..., None]
    difference = mix_first - lambdas.reshape(kv_here, per_kv, 1, 1) * mix_second
    mean_sq = jnp.mean(difference * difference, axis=-1, keepdims=True)
    normed_heads = (difference * lax.rsqrt(mean_sq + EPS) * head_gain * OUT_SCALE).astype(
        jnp.bfloat16
    )
    heads_out = normed_heads.transpose(2, 0, 1, 3).reshape(rows_q, heads_here * VAL_DIM)
    rows_here = stream_in.shape[0]
    picked_rows = heads_out
    attended = sum_at_owner(
        jnp.dot(picked_rows, out_weight, preferred_element_type=jnp.float32).astype(jnp.bfloat16),
        "tp",
        0,
    )
    stream = stream_in.astype(jnp.float32) + attended
    normed = (
        stream * lax.rsqrt(jnp.mean(stream * stream, axis=-1, keepdims=True) + EPS) * norm_gain
    ).astype(jnp.bfloat16)
    top_count = expert_ids.shape[1]
    experts_all = lax.axis_size("sp")
    slot_cap = 2 * top_count * rows_here // experts_all
    flat_ids = expert_ids.reshape(-1)
    one_hot = (flat_ids[:, None] == lax.iota(jnp.int32, experts_all)[None, :]).astype(jnp.int32)
    ranks = jnp.sum((jnp.cumsum(one_hot, axis=0) - 1) * one_hot, axis=1)
    slots = flat_ids * slot_cap + ranks
    selector = (slots[None, :] == lax.iota(jnp.int32, experts_all * slot_cap)[:, None]).astype(
        jnp.bfloat16
    )
    selector = jnp.sum(selector.reshape(experts_all * slot_cap, rows_here, top_count), axis=2)
    send_rows = jnp.dot(selector, normed, preferred_element_type=jnp.float32).astype(jnp.bfloat16)
    received = lax.all_to_all(send_rows, "sp", split_axis=0, concat_axis=0, tiled=True)
    all_rows = lax.all_gather(received, "tp", axis=0, tiled=True)
    picked_rows = all_rows
    gate = jnp.dot(picked_rows, gate_weight[0], preferred_element_type=jnp.float32)
    upper = jnp.dot(picked_rows, up_weight[0], preferred_element_type=jnp.float32)
    hidden = (jax.nn.silu(gate) * upper).astype(jnp.bfloat16)
    summed = lax.psum_scatter(
        jnp.dot(hidden, down_weight[0], preferred_element_type=jnp.float32).astype(jnp.bfloat16),
        "tp",
        scatter_dimension=0,
        tiled=True,
    )
    returned = lax.all_to_all(summed, "sp", split_axis=0, concat_axis=0, tiled=True)
    picked = jnp.take(returned, slots, axis=0).reshape(rows_here, top_count, -1).astype(jnp.float32)
    routed = jnp.sum(picked * route_weight[:, :, None], axis=1)
    return (stream + routed).astype(jnp.bfloat16)


def solution(mesh):
    return jax.shard_map(
        shards,
        mesh=mesh,
        in_specs=(
            P(("sp", "tp"), None),
            P("sp", "tp"),
            P("sp", "tp"),
            P("sp", "tp"),
            P("sp", "tp"),
            P("sp", "tp"),
            P("tp"),
            P(),
            P("tp", None),
            P(),
            P(("sp", "tp"), None),
            P(("sp", "tp"), None),
            P("sp", None, "tp"),
            P("sp", None, "tp"),
            P("sp", "tp", None),
        ),
        out_specs=P(("sp", "tp"), None),
        check_vma=False,
    )
```

profile of v0, /device:TPU:1, one launch (start us, length us, event | category | flops | bytes accessed | tf_op | source)
XLA Modules:
  0.0 467.8 jit_solution(7342264499680508700)
XLA Ops:
  6.5 1.8 pad_maximum_fusion
  11.4 102.2 %all-gather.3.cloned.1.call-done = bf16[16384,512]{1,0:T(8,128)(2,1)} async-done(((bf16[256,512]{1,0:T(8,128)(2,1)}), bf16[16384,512]{1,0:T(8,128)(2,1)}) %all-gather.3.cloned.1.call-update) | async-done | bytes 16777232 | tf_op jit(solution)/shard_map/all_gather | solution.py:108
  113.7 19.9 %while.24 = (s32[]{:T(128)}, f32[1,2,256]{2,1,0:T(2,128)S(1)}, f32[1,2,256]{2,1,0:T(2,128)S(1)}, f32[1,2,256,256]{3,2,1,0:T(8,128)S(1)}, f32[1,2,256]{2,1,0:T(2,...) while((s32[]{:T(128)}, f32[1,2,256]{2,1,0:T(2,128)S(1)}, ...), condition=%wide.region_8.9_spmd.clone, body=%wide.region_1.8_spmd.clone.sunk | while | flops 813707520 | bytes 17390044 | solution.py:72
  114.4 7.3 %conditional.3 = (f32[1,2,256]{2,1,0:T(2,128)S(1)}, f32[1,2,256]{2,1,0:T(2,128)S(1)}, f32[1,2,256,256]{3,2,1,0:T(8,128)S(1)}, f32[1,2,256]{2,1,0:T(2,128)S(1)}, ...) conditional(s32[]{:T(128)} %convert_element_type.98, (s32[]{:T(128)}, s32[]{:T(128)}, s32[]{:T(128)}, ...), branch_computations={%region_2.6_spmd, %region_7.7_spmd} | conditional | flops 813707520 | bytes 17380510 | solution.py:70
  114.8 1.4 fusion.43
  116.6 1.7 fusion.7
  118.2 1.4 fusion.42
  119.7 1.7 fusion.6
  136.2 1.7 convolution_convert_fusion.1
  137.9 4.1 all-to-all-start
  143.1 13.6 %all-to-all-done = bf16[4,64,2048]{2,1,0:T(8,128)(2,1)S(1)} async-done(((bf16[4,64,2048]{2,1,0:T(8,128)(2,1)}), bf16[4,64,2048]{2,1,0:T(8,128)(2,1)S(1)}, u32[]{:S(2)}, u32[]{:S(2)}) %all-to-all-start) | async-done | bytes 1048608 | tf_op jit(solution)/shard_map/all_to_all | solution.py:23
  158.1 1.2 all_to_all.20
  159.4 142.1 %all_to_all.29 = bf16[64,4,2048]{2,1,0:T(4,128)(2,1)S(1)} all-to-all(bf16[64,4,2048]{2,1,0:T(4,128)(2,1)} %all_to_all.20), channel_id=1, replica_groups=mesh['sp'=64,'tp'=4] {'sp'}, dimensions={0} | all-to-all | bytes 2097152 | tf_op jit(solution)/shard_map/all_to_all | solution.py:145
  302.9 45.5 %all-gather.5.cloned.1.call-done = bf16[1024,2048]{1,0:T(8,128)(2,1)} async-done(((bf16[256,2048]{1,0:T(8,128)(2,1)}), bf16[1024,2048]{1,0:T(8,128)(2,1)}) %all-gather.5.cloned.1.call-update) | async-done | bytes 4194320 | tf_op jit(solution)/shard_map/all_gather | solution.py:146
  348.4 4.8 %fusion.25 = f32[1024,256]{1,0:T(8,128)} fusion(bf16[1024,2048]{1,0:T(8,128)(2,1)} %all-gather.5.cloned.1.call-done, bf16[1,2048,256]{2,1,0:T(8,128)(2,1)} %param.31), kind=kOutput, calls=%fused_computation.48 | convolution fusion | flops 1073741824 | bytes 6291456 | tf_op jit(solution)/shard_map/dot_general | solution.py:148
  353.2 9.1 %convolution_convert_fusion = bf16[1024,2048]{1,0:T(8,128)(2,1)} fusion(bf16[1024,2048]{1,0:T(8,128)(2,1)} %all-gather.5.cloned.1.call-done, bf16[1,256,2048]{2,1,0:T(8,128)(2,1)S(1)} %copy-done.9, bf16[1,2048,256]{2,1,0:T(8,128)(2,1)} %param.32, f32[1024,256]{1,0:T(8,128)} %fusion.25), kind=kOutput, calls=%fused_computation.40 | convolution fusion | flops 2151153664 | bytes 11534336 | tf_op jit(solution)/shard_map/dot_general | solution.py:152
  362.4 50.0 %reduce-scatter.2.cloned.1.call-done = bf16[256,2048]{1,0:T(8,128)(2,1)} async-done(((bf16[1024,2048]{1,0:T(8,128)(2,1)}), bf16[256,2048]{1,0:T(8,128)(2,1)}) %reduce-scatter.2.cloned.1.call-update) | async-done | bytes 1048592 | tf_op jit(solution)/shard_map/reduce_scatter | solution.py:151
  412.4 2.3 all_to_all.23
  414.6 10.9 %all-to-all-start.2 = ((bf16[64,4,2048]{2,1,0:T(4,128)(2,1)}), bf16[64,4,2048]{2,1,0:T(4,128)(2,1)}, u32[]{:S(2)}, u32[]{:S(2)}) async-start(bf16[64,4,2048]{2,1,0:T(4,128)(2,1)} %all_to_all.23), calls=%async_computation.3 | async-start | bytes 2097152 | tf_op jit(solution)/shard_map/all_to_all | solution.py:157
  426.1 27.6 %all-to-all-done.2 = bf16[64,4,2048]{2,1,0:T(4,128)(2,1)} async-done(((bf16[64,4,2048]{2,1,0:T(4,128)(2,1)}), bf16[64,4,2048]{2,1,0:T(4,128)(2,1)}, u32[]{:S(2)}, u32[]{:S(2)}) %all-to-all-start.2) | async-done | bytes 1048608 | tf_op jit(solution)/shard_map/all_to_all | solution.py:157
  453.7 1.3 all_to_all.25
  455.0 1.7 gather_fusion
  456.7 1.4 gather.7
  458.2 2.3 multiply_reduce_fusion
  (168 shorter events, 12.5 us)
Async XLA Ops:
  6.5 129.7 %copy-start = (bf16[512,2048]{1,0:T(8,128)(2,1)S(1)}, bf16[512,2048]{1,0:T(8,128)(2,1)}, u32[]{:S(2)}) copy-start(bf16[512,2048]{1,0:T(8,128)(2,1)} %param.27) | copy-start | bytes 6291460
  6.5 107.1 %all-gather.3.cloned.1.call-start = ((), (), s32[]{:S(2)}) async-start(), calls=%async_computation.4 | async-start | bytes 17039360 | tf_op jit(solution)/shard_map/all_gather | solution.py:108
  133.6 1.2 copy-start.8
  133.6 2.4 copy-start.6
  136.2 5.8 %copy-start.4 = (s32[64,2]{0,1:T(2,128)S(1)}, s32[64,2]{0,1:T(2,128)}, u32[]{:S(2)}) copy-start(s32[64,2]{0,1:T(2,128)} %param.29) | copy-start | bytes 1540
  137.9 18.9 %copy-start.3 = (bf16[64,2048]{1,0:T(8,128)(2,1)S(1)}, bf16[64,2048]{1,0:T(8,128)(2,1)}, u32[]{:S(2)}) copy-start(bf16[64,2048]{1,0:T(8,128)(2,1)} %param.19) | copy-start | bytes 786436
  137.9 19.7 %copy-start.5 = (f32[2048]{0:T(1024)S(1)}, f32[2048]{0:T(1024)}, u32[]{:S(2)}) copy-start(f32[2048]{0:T(1024)} %param.28) | copy-start | bytes 24580
  137.9 18.7 %all-to-all-start = ((bf16[4,64,2048]{2,1,0:T(8,128)(2,1)}), bf16[4,64,2048]{2,1,0:T(8,128)(2,1)S(1)}, u32[]{:S(2)}, u32[]{:S(2)}) async-start(bf16[4,64,2048]{2,1,0:T(8,128)(2,1)} %bitcast.93), calls=%async_computation | async-start | bytes 2097152 | tf_op jit(solution)/shard_map/all_to_all | solution.py:23
  142.0 206.4 %all-gather.5.cloned.1.call-start = ((), (), s32[]{:S(2)}) async-start(), calls=%async_computation.5 | async-start | bytes 5242880 | tf_op jit(solution)/shard_map/all_gather | solution.py:146
  156.9 0.8 copy-start.1
  302.6 50.6 %copy-start.9 = (bf16[1,256,2048]{2,1,0:T(8,128)(2,1)S(1)}, bf16[1,256,2048]{2,1,0:T(8,128)(2,1)}, u32[]{:S(2)}) copy-start(bf16[1,256,2048]{2,1,0:T(8,128)(2,1)} %param.33) | copy-start | bytes 3145732
  302.7 109.7 %reduce-scatter.2.cloned.1.call-start = ((), (), s32[]{:S(2)}) async-start(), calls=%async_computation.6 | async-start | bytes 5242880 | tf_op jit(solution)/shard_map/reduce_scatter | solution.py:151
  362.3 63.5 %copy-start.7 = (f32[64,2]{0,1:T(2,128)S(1)}, f32[64,2]{0,1:T(2,128)}, u32[]{:S(2)}) copy-start(f32[64,2]{0,1:T(2,128)} %param.30) | copy-start | bytes 1540
  414.6 39.0 %all-to-all-start.2 = ((bf16[64,4,2048]{2,1,0:T(4,128)(2,1)}), bf16[64,4,2048]{2,1,0:T(4,128)(2,1)}, u32[]{:S(2)}, u32[]{:S(2)}) async-start(bf16[64,4,2048]{2,1,0:T(4,128)(2,1)} %all_to_all.23), calls=%async_computation.3 | async-start | bytes 2097152 | tf_op jit(solution)/shard_map/all_to_all | solution.py:157
  456.7 3.8 copy-start.2
Sparse Core Ops, SparseCore 0:
  10.1 103.4 all-gather.2
  302.8 45.6 all-gather.4
  362.5 49.8 reduce-scatter.1
where the time goes:
time: 471 us; the launch traced here: 468 us
  waiting for transfers between devices  239 us (51%)
  blocking collectives  142 us (30%)
  matrix products  22.3 us (5%)
  starting transfers between devices  15.3 us (3%)
  local copies, waits for them, and re-layouts  14.3 us (3%)
  between operations  13.4 us (3%)
  loops' own time  12.5 us (3%)
  other arithmetic  8.84 us (2%)
    all_to_all x1, blocking collectives, shards(): lax.all_to_all(send_rows, 'sp', split_axis=0, concat_axis=0, tiled=True)  142 us
    all_gather x1, waiting for transfers between devices, shards(): lax.all_gather(packed, 'sp', axis=0, tiled=True)  102 us
    reduce_scatter x1, waiting for transfers between devices, shards(): lax.psum_scatter(jnp.dot(hidden, down_weight[0], preferred_element_type=j...  50 us
    all_gather x1, waiting for transfers between devices, shards(): all_rows = lax.all_gather(received, 'tp', axis=0, tiled=True)  45.5 us
    all_to_all x1, waiting for transfers between devices, shards(): lax.all_to_all(summed, 'sp', split_axis=0, concat_axis=0, tiled=True)  27.6 us
    all_to_all x1, waiting for transfers between devices, sum_at_owner(): tiles = lax.all_to_all(cut_along(x, dim, peers), axis, 0, 0, tiled=True)  13.6 us
    another operation x1, loops' own time, fold_piece(): return lax.fori_loop(0, num_blocks, advance, carried)  11.8 us
    all_to_all x1, starting transfers between devices, shards(): lax.all_to_all(summed, 'sp', split_axis=0, concat_axis=0, tiled=True)  10.9 us
  transfers between devices with their start and end apart: 5, of which 5 were waited for; matrix products, arithmetic and copies ran while one was open for 1% of the time, Pallas kernels for 0%

commit v1 on v0

v1 whole, which is shorter than its diff:
```python
import functools
import math

import jax
import jax.numpy as jnp
from jax import lax
from jax.experimental import pallas as pl
from jax.experimental.pallas import tpu as pltpu
from jax.sharding import Mesh
from jax.sharding import PartitionSpec as P


HEAD_DIM = 128
VAL_DIM = 256
LANES = 128

EPS = 1e-06
OUT_SCALE = 0.8
LOW = -1e30
EXP2_SCALE = HEAD_DIM ** (-0.5) * math.log2(math.e)

PARTS = 2
KEY_STEP = 512
CHAIN_ROWS = 512


def lanes_to(x, width):
    return jnp.concatenate([x] * (width // LANES), axis=1)


def attend_kernel(first, last, rows, part, part_rows, key_step, *refs):
    info, q_one_own, q_one_other, q_two_own, q_two_other, kv = refs[:6]
    refs = refs[6:]
    if not first:
        acc_in, max_in, sum_in = refs[:3]
        refs = refs[3:]
    if last:
        own_acc, own_stats, other_acc, other_stats, q_all, acc, row_max, row_sum = refs
    else:
        acc, row_max, row_sum, q_all = refs
    chip = info[0]
    core = info[1]
    step = pl.program_id(0)
    group = key_step // part_rows
    last_step = chip // group
    map_rows = 4 * rows

    @pl.when(step == 0)
    def _():
        for a, pieces in enumerate(((q_one_own, q_one_other), (q_two_own, q_two_other))):
            for h in range(2):
                for t in range(2):
                    start = a * map_rows + (2 * h + t) * rows
                    q_all[start : start + rows, :] = pieces[t][:, h * HEAD_DIM : (h + 1) * HEAD_DIM]
        if first:
            acc[...] = jnp.zeros_like(acc)
            row_max[...] = jnp.full(row_max.shape, LOW, jnp.float32)
            row_sum[...] = jnp.zeros_like(row_sum)
        else:
            acc[...] = acc_in[...]
            row_max[...] = max_in[...]
            row_sum[...] = sum_in[...]

    chain = min(CHAIN_ROWS, map_rows)

    def fold(a, start, masked):
        at = pl.ds(start, chain)
        keys = kv[:, a * HEAD_DIM : (a + 1) * HEAD_DIM]
        scores = lax.dot_general(
            q_all[at, :], keys, (((1,), (1,)), ((), ())), preferred_element_type=jnp.float32
        )
        if masked:
            row = lax.broadcasted_iota(jnp.int32, (chain, 1), 0) + start
            piece = (row // rows) % 2
            query = (2 * chip + jnp.where(piece == 0, core, 1 - core)) * rows + row % rows
            col = lax.broadcasted_iota(jnp.int32, (1, key_step), 1)
            holder = step * group + col // part_rows
            key = (2 * holder + core) * rows + part * part_rows + col % part_rows
            scores = jnp.where(key <= query, scores, LOW)
        old_max = row_max[at, :]
        new_max = jnp.maximum(old_max, jnp.max(scores, axis=1, keepdims=True))
        terms = jnp.exp2(scores * EXP2_SCALE - lanes_to(new_max * EXP2_SCALE, key_step))
        rescale = jnp.exp2((old_max - new_max) * EXP2_SCALE)
        row_max[at, :] = new_max
        part_sum = terms[:, :LANES]
        for j in range(1, key_step // LANES):
            part_sum = part_sum + terms[:, j * LANES : (j + 1) * LANES]
        row_sum[at, :] = row_sum[at, :] * rescale + part_sum
        mixed = jnp.dot(
            terms.astype(jnp.bfloat16), kv[:, 2 * HEAD_DIM :], preferred_element_type=jnp.float32
        )
        acc[at, :] = acc[at, :] * lanes_to(rescale, VAL_DIM) + mixed

    @pl.when(step < last_step)
    def _():
        for start in range(0, 2 * map_rows, chain):
            fold(start // map_rows, start, False)

    @pl.when(step == last_step)
    def _():
        for a in range(2):

            def masked_chain(i, _):
                fold(a, pl.multiple_of(a * map_rows + i * chain, chain), True)
                return 0

            lax.fori_loop(0, map_rows // chain, masked_chain, 0)

    if last:

        @pl.when(step == pl.num_programs(0) - 1)
        def _():
            lane = lax.broadcasted_iota(jnp.int32, (rows, LANES), 1)
            for t, (acc_out, stats_out) in enumerate(
                ((own_acc, own_stats), (other_acc, other_stats))
            ):
                stats = jnp.zeros((rows, LANES), jnp.float32)
                for k in range(4):
                    start = (2 * k + t) * rows
                    at = slice(start, start + rows)
                    acc_out[k * rows : (k + 1) * rows, :] = acc[at, :].astype(acc_out.dtype)
                    total = jnp.sum(row_sum[at, :], axis=1, keepdims=True)
                    stats = jnp.where(lane == k, row_max[at, :], stats)
                    stats = jnp.where(lane == 4 + k, total, stats)
                stats_out[...] = stats


def attend(info, queries, kv, state, part, parts):
    first, last = state is None, part == parts - 1
    rows = queries[0].shape[0]
    part_rows = rows // parts
    key_step = min(KEY_STEP, kv.shape[0])
    group = key_step // part_rows
    steps = kv.shape[0] // key_step
    whole = lambda shape: pl.BlockSpec(shape, lambda i, info: (0,) * len(shape))
    state_shapes = [
        jax.ShapeDtypeStruct((8 * rows, VAL_DIM), jnp.float32),
        jax.ShapeDtypeStruct((8 * rows, LANES), jnp.float32),
        jax.ShapeDtypeStruct((8 * rows, LANES), jnp.float32),
    ]
    q_scratch = pltpu.VMEM((8 * rows, HEAD_DIM), jnp.bfloat16)
    if last:
        out_shape = [
            jax.ShapeDtypeStruct((4 * rows, VAL_DIM), jnp.float32),
            jax.ShapeDtypeStruct((rows, LANES), jnp.float32),
            jax.ShapeDtypeStruct((4 * rows, VAL_DIM), jnp.bfloat16),
            jax.ShapeDtypeStruct((rows, LANES), jnp.float32),
        ]
        scratch = [q_scratch] + [pltpu.VMEM(s.shape, s.dtype) for s in state_shapes]
    else:
        out_shape = state_shapes
        scratch = [q_scratch]
    operands = list(queries) + [kv] + ([] if first else list(state))
    in_specs = [whole(q.shape) for q in queries]
    in_specs.append(
        pl.BlockSpec((key_step, kv.shape[1]), lambda i, info: (jnp.minimum(i, info[0] // group), 0))
    )
    if not first:
        in_specs += [whole(s.shape) for s in state_shapes]
    pairs = 8 * rows * kv.shape[0]
    return pl.pallas_call(
        functools.partial(attend_kernel, first, last, rows, part, part_rows, key_step),
        out_shape=out_shape,
        grid_spec=pltpu.PrefetchScalarGridSpec(
            num_scalar_prefetch=1,
            grid=(steps,),
            in_specs=in_specs,
            out_specs=[whole(s.shape) for s in out_shape],
            scratch_shapes=scratch,
        ),
        compiler_params=pltpu.CompilerParams(
            dimension_semantics=("arbitrary",), vmem_limit_bytes=28 * 1024 * 1024
        ),
        cost_estimate=pl.CostEstimate(
            flops=2 * pairs * (HEAD_DIM + VAL_DIM), transcendentals=pairs, bytes_accessed=kv.size * 2
        ),
    )(info, *operands)


def project_kernel(
    rows, lambdas, gain, own_acc, own_stats, other_acc, other_stats, weight, out
):
    stats_a, stats_b = own_stats[...], other_stats[...]

    def mix(k):
        at = slice(k * rows, (k + 1) * rows)
        max_a, max_b = stats_a[:, k : k + 1], stats_b[:, k : k + 1]
        top = jnp.maximum(max_a, max_b)
        share_a = jnp.exp2((max_a - top) * EXP2_SCALE)
        share_b = jnp.exp2((max_b - top) * EXP2_SCALE)
        total = stats_a[:, 4 + k : 5 + k] * share_a + stats_b[:, 4 + k : 5 + k] * share_b
        mixed = own_acc[at, :] * share_a + other_acc[at, :].astype(jnp.float32) * share_b
        return mixed / total

    heads = []
    for h in range(2):
        difference = mix(h) - lambdas[h] * mix(2 + h)
        mean_sq = jnp.mean(difference * difference, axis=-1, keepdims=True)
        normed = difference * lax.rsqrt(mean_sq + EPS) * gain[...] * OUT_SCALE
        heads.append(normed.astype(jnp.bfloat16))
    heads_out = jnp.concatenate(heads, axis=1)
    out[...] = jnp.dot(heads_out, weight[...], preferred_element_type=jnp.float32).astype(
        jnp.bfloat16
    )


def project(lambdas, head_gain, own_acc, own_stats, other_acc, other_stats, out_weight):
    rows = own_stats.shape[0]
    vmem = pl.BlockSpec(memory_space=pltpu.VMEM)
    return pl.pallas_call(
        functools.partial(project_kernel, rows),
        out_shape=jax.ShapeDtypeStruct((rows, out_weight.shape[1]), jnp.bfloat16),
        in_specs=[pl.BlockSpec(memory_space=pltpu.SMEM)] + [vmem] * 6,
        out_specs=vmem,
        compiler_params=pltpu.CompilerParams(vmem_limit_bytes=32 * 1024 * 1024),
        cost_estimate=pl.CostEstimate(
            flops=2 * rows * out_weight.size, transcendentals=0, bytes_accessed=out_weight.size * 2
        ),
        name="project",
    )(lambdas, head_gain.reshape(1, -1), own_acc, own_stats, other_acc, other_stats, out_weight)


def dispatch_kernel(tiles, stream_in, gain, selector, stream_out, send):
    attended = tiles[0].astype(jnp.float32)
    for t in range(1, tiles.shape[0]):
        attended = attended + tiles[t].astype(jnp.float32)
    stream = stream_in[...].astype(jnp.float32) + attended
    stream_out[...] = stream
    mean_sq = jnp.mean(stream * stream, axis=-1, keepdims=True)
    normed = (stream * lax.rsqrt(mean_sq + EPS) * gain[...]).astype(jnp.bfloat16)
    send[...] = jnp.dot(selector[...], normed, preferred_element_type=jnp.float32).astype(
        jnp.bfloat16
    )


def dispatch(tiles, stream_in, norm_gain, selector):
    rows, width = stream_in.shape
    vmem = pl.BlockSpec(memory_space=pltpu.VMEM)
    return pl.pallas_call(
        dispatch_kernel,
        out_shape=[
            jax.ShapeDtypeStruct((rows, width), jnp.float32),
            jax.ShapeDtypeStruct((selector.shape[0], width), jnp.bfloat16),
        ],
        in_specs=[vmem] * 4,
        out_specs=[vmem] * 2,
        cost_estimate=pl.CostEstimate(
            flops=2 * selector.size * width, transcendentals=0, bytes_accessed=4 * tiles.size
        ),
        name="dispatch",
    )(tiles, stream_in, norm_gain.reshape(1, -1), selector)


def experts_kernel(rows_in, *refs):
    sources, (out, gate, up, down, sums, sems) = refs[:16], refs[16:]
    half = rows_in.shape[1] // 2
    copies = []
    for g in range(4):
        gate_from, up_low, up_high, down_from = sources[4 * g : 4 * g + 4]
        copies.append(
            [
                (gate_from, gate.at[g]),
                (up_low, up.at[g, :half, :]),
                (up_high, up.at[g, half:, :]),
                (down_from, down.at[g]),
            ]
        )
    started = []
    for group in copies:
        started.append([])
        for source, target in group:
            number = sum(map(len, started))
            copy = pltpu.make_async_copy(source, target, sems.at[number])
            copy.start()
            started[-1].append(copy)
    for g, group in enumerate(started):
        for copy in group[:-1]:
            copy.wait()
        picked = rows_in[...]
        gated = jnp.dot(picked, gate[g], preferred_element_type=jnp.float32)
        upper = jnp.dot(picked, up[g], preferred_element_type=jnp.float32)
        hidden = (gated / (1.0 + jnp.exp(-gated)) * upper).astype(jnp.bfloat16)
        group[-1].wait()
        piece = jnp.dot(hidden, down[g], preferred_element_type=jnp.float32)
        if g == 0:
            sums[...] = piece
        elif g < 3:
            sums[...] = sums[...] + piece
        else:
            out[...] = (sums[...] + piece).astype(jnp.bfloat16)


def experts(rows_in, weights):
    rows, width = rows_in.shape
    units = weights[0].shape[1]
    vmem = pl.BlockSpec(memory_space=pltpu.VMEM)
    return pl.pallas_call(
        experts_kernel,
        out_shape=jax.ShapeDtypeStruct((rows, width), jnp.bfloat16),
        in_specs=[vmem] + [pl.BlockSpec(memory_space=pl.ANY)] * 16,
        out_specs=vmem,
        scratch_shapes=[
            pltpu.VMEM((4, width, units), jnp.bfloat16),
            pltpu.VMEM((4, width, units), jnp.bfloat16),
            pltpu.VMEM((4, units, width), jnp.bfloat16),
            pltpu.VMEM((rows, width), jnp.float32),
            pltpu.SemaphoreType.DMA((16,)),
        ],
        compiler_params=pltpu.CompilerParams(vmem_limit_bytes=40 * 1024 * 1024),
        cost_estimate=pl.CostEstimate(
            flops=24 * rows * width * units, transcendentals=4 * rows * units, bytes_accessed=24 * width * units
        ),
        name="experts",
    )(rows_in, *weights)


def collect_kernel(returned, choice_one, choice_two, route_weight, stream, out):
    picked_one = jnp.dot(choice_one[...], returned[...], preferred_element_type=jnp.float32)
    picked_two = jnp.dot(choice_two[...], returned[...], preferred_element_type=jnp.float32)
    routed = picked_one * route_weight[:, 0:1] + picked_two * route_weight[:, 1:2]
    out[...] = (stream[...] + routed).astype(jnp.bfloat16)


def collect(returned, choice_one, choice_two, route_weight, stream):
    vmem = pl.BlockSpec(memory_space=pltpu.VMEM)
    return pl.pallas_call(
        collect_kernel,
        out_shape=jax.ShapeDtypeStruct(stream.shape, jnp.bfloat16),
        in_specs=[vmem] * 5,
        out_specs=vmem,
        cost_estimate=pl.CostEstimate(
            flops=4 * choice_one.size * stream.shape[1], transcendentals=0, bytes_accessed=2 * returned.size
        ),
        name="collect",
    )(returned, choice_one, choice_two, route_weight, stream)


def body(
    stream_in,
    queries_one,
    queries_two,
    keys_one,
    keys_two,
    values,
    lambdas,
    head_gain,
    out_weight,
    norm_gain,
    expert_ids,
    route_weight,
    gate_weight,
    up_weight,
    down_weight,
):
    rows_q = queries_one.shape[0]
    chip = lax.axis_index("chip")
    core = lax.axis_index("core")
    peers = lax.axis_size("tp")

    part_rows = rows_q // PARTS
    gathered = []
    for i in range(PARTS):
        at = slice(i * part_rows, (i + 1) * part_rows)
        packed = jnp.concatenate([keys_one[at], keys_two[at], values[at]], 1)
        gathered.append(lax.all_gather(packed, "chip", axis=0, tiled=True))
    swap = [(0, 1), (1, 0)]
    other_one = lax.ppermute(queries_one, "core", swap)
    other_two = lax.ppermute(queries_two, "core", swap)

    up_ring = [(i, (i + 1) % peers) for i in range(peers)]
    down_ring = [(i, (i - 1) % peers) for i in range(peers)]
    half = up_weight.shape[1] // 2
    own = [gate_weight[0], up_weight[0, :half], up_weight[0, half:], down_weight[0]]
    below = [lax.ppermute(w, "tp", up_ring) for w in own]
    above = [lax.ppermute(w, "tp", down_ring) for w in own]
    across = [lax.ppermute(w, "tp", up_ring) for w in below[:2]]
    across += [lax.ppermute(w, "tp", down_ring) for w in above[2:]]
    weights = [*own, *below, *above, *across]

    rows_here = stream_in.shape[0]
    top_count = expert_ids.shape[1]
    experts_all = lax.axis_size("chip") * lax.axis_size("core")
    slot_cap = 2 * top_count * rows_here // experts_all
    flat_ids = expert_ids.reshape(-1)
    one_hot = (flat_ids[:, None] == lax.iota(jnp.int32, experts_all)[None, :]).astype(jnp.int32)
    ranks = jnp.sum((jnp.cumsum(one_hot, axis=0) - 1) * one_hot, axis=1)
    slots = (flat_ids * slot_cap + ranks).reshape(rows_here, top_count)
    all_slots = lax.iota(jnp.int32, experts_all * slot_cap)
    choice_one = (slots[:, 0:1] == all_slots[None, :]).astype(jnp.bfloat16)
    choice_two = (slots[:, 1:2] == all_slots[None, :]).astype(jnp.bfloat16)
    selector = (choice_one + choice_two).T

    info = jnp.stack([chip, core]).astype(jnp.int32)
    info, choice_one, choice_two, selector = lax.optimization_barrier(
        (info, choice_one, choice_two, selector)
    )
    queries = (queries_one, other_one, queries_two, other_two)
    state = None
    for i in range(PARTS):
        state = attend(info, queries, gathered[i], state, i, PARTS)
    own_acc, own_stats, other_acc, other_stats = state
    from_acc = lax.ppermute(other_acc, "core", swap)
    from_stats = lax.ppermute(other_stats, "core", swap)
    partial_rows = project(
        lambdas, head_gain, own_acc, own_stats, from_acc, from_stats, out_weight
    )
    tiles = lax.all_to_all(
        partial_rows.reshape(peers, rows_here, -1), "tp", 0, 0, tiled=True
    )
    stream, send_rows = dispatch(tiles, stream_in, norm_gain, selector)
    received = lax.all_to_all(send_rows, ("chip", "core"), split_axis=0, concat_axis=0, tiled=True)
    results = experts(received, weights)
    returned = lax.all_to_all(results, ("chip", "core"), split_axis=0, concat_axis=0, tiled=True)
    return collect(returned, choice_one, choice_two, route_weight, stream)


def solution(mesh):
    sp, tp = mesh.devices.shape
    split = Mesh(mesh.devices.reshape(sp // 2, 2, tp), ("chip", "core", "tp"))
    sp_axes = ("chip", "core")
    everywhere = ("chip", "core", "tp")
    return jax.shard_map(
        body,
        mesh=split,
        in_specs=(
            P(everywhere, None),
            P(sp_axes, "tp"),
            P(sp_axes, "tp"),
            P(sp_axes, "tp"),
            P(sp_axes, "tp"),
            P(sp_axes, "tp"),
            P("tp"),
            P(),
            P("tp", None),
            P(),
            P(everywhere, None),
            P(everywhere, None),
            P(sp_axes, None, "tp"),
            P(sp_axes, None, "tp"),
            P(sp_axes, "tp", None),
        ),
        out_specs=P(everywhere, None),
        check_vma=False,
    )
```

time: 471 us -> 389 us (0.83)
  blocking collectives: 142 us -> 0 us
  starting transfers between devices: 15.3 us -> 62.7 us
  Pallas kernels: 0 us -> 25.3 us
  matrix products: 22.3 us -> 0 us
  local copies, waits for them, and re-layouts: 14.3 us -> 28.7 us
  waiting for transfers between devices: 239 us -> 253 us
  loops' own time: 12.5 us -> 0 us
  other arithmetic: 8.84 us -> 3.9 us
    all_to_all x1 -> x0, blocking collectives: 142 us -> none  [shards(): lax.all_to_all(send_rows, 'sp', split_axis=0, concat_axis=0, tiled=True)]
    ppermute x0 -> x16, waiting for transfers between devices: none -> 69.9 us  [the longest x2 26.7 us: body(): across += [lax.ppermute(w, 'tp', down_ring) for w in above[2:]]]
    reduce_scatter x1 -> x0, waiting for transfers between devices: 50 us -> none  [shards(): lax.psum_scatter(jnp.dot(hidden, down_weight[0], preferred_element_type=j...]
    all_to_all x2 -> x3, starting transfers between devices: 15 us -> 41.2 us  [the longest x1 20.1 us: body(): lax.all_to_all(send_rows, ('chip', 'core'), split_axis=0, concat_axis=0,...]
    pallas_call x0 -> x6, Pallas kernels: none -> 25.3 us  [the longest x2 10.7 us: attend(): pl.pallas_call(functools.partial(attend_kernel, first, last, rows, part,...]
    dot_general x8 -> x0, matrix products: 22.3 us -> none  [the longest x1 9.1 us: shards(): jnp.dot(hidden, down_weight[0], preferred_element_type=jnp.float32)]
    ppermute x0 -> x16, starting transfers between devices: none -> 21.5 us  [the longest x4 6.65 us: body(): above = [lax.ppermute(w, 'tp', down_ring) for w in own]]
    unnamed x26 -> x52, local copies, waits for them, and re-layouts: 3.09 us -> 20.7 us
  transfers between devices with their start and end apart: 5 -> 21, of which waited for: 5 -> 10; matrix products, arithmetic and copies ran while one was open for 1% -> 1% of each run, Pallas kernels for 0% -> 2%
where the time goes in v1:
time: 389 us; the launch traced here: 388 us
  waiting for transfers between devices  253 us (65%)
  starting transfers between devices  62.7 us (16%)
  local copies, waits for them, and re-layouts  28.7 us (7%)
  Pallas kernels  25.3 us (7%)
  between operations  13.6 us (3%)
  other arithmetic  3.9 us (1%)
    all_gather x2, waiting for transfers between devices, body(): gathered.append(lax.all_gather(packed, 'chip', axis=0, tiled=True))  145 us
    all_to_all x1, waiting for transfers between devices, body(): lax.all_to_all(results, ('chip', 'core'), split_axis=0, concat_axis=0, ti...  27.5 us
    ppermute x2, waiting for transfers between devices, body(): across += [lax.ppermute(w, 'tp', down_ring) for w in above[2:]]  26.7 us
    ppermute x2, waiting for transfers between devices, body(): across = [lax.ppermute(w, 'tp', up_ring) for w in below[:2]]  22.9 us
    unnamed x52, local copies, waits for them, and re-layouts  20.7 us
    all_to_all x1, starting transfers between devices, body(): lax.all_to_all(send_rows, ('chip', 'core'), split_axis=0, concat_axis=0,...  20.1 us
    all_to_all x1, starting transfers between devices, body(): lax.all_to_all(results, ('chip', 'core'), split_axis=0, concat_axis=0, ti...  16.8 us
    ppermute x4, waiting for transfers between devices, body(): above = [lax.ppermute(w, 'tp', down_ring) for w in own]  13 us
  transfers between devices with their start and end apart: 21, of which 10 were waited for; matrix products, arithmetic and copies ran while one was open for 1% of the time, Pallas kernels for 2%

profile of v1, /device:TPU:1, one launch (start us, length us, event | category | flops | bytes accessed | tf_op | source)
XLA Modules:
  0.0 387.7 jit_solution(17850849618859402524)
XLA Ops:
  9.7 3.3 collective-permute-start
  16.8 75.3 %all-gather.5.cloned.1.call-done.refs_5_ = bf16[4096,512]{1,0:T(8,128)(2,1)} async-done(((bf16[128,512]{1,0:T(8,128)(2,1)}), bf16[4096,512]{1,0:T(8,128)(2,1)}) %all-gather.5.cloned.1.call-update) | async-done | bytes 4194320 | tf_op jit(solution)/shard_map/all_gather | solution.py:365
  92.1 2.2 copy-done.13
  96.1 5.1 %shard_map.145 = (f32[2048,256]{1,0:T(8,128)S(1)}, f32[2048,128]{1,0:T(8,128)S(1)}, f32[2048,128]{1,0:T(8,128)S(1)}) custom-call(s32[2]{0:T(128)S(1)} %pad_add_fusion.refs_0_, bf16[256,256]{1,0:T(8,128)(2,1)S(1)} %copy-done.15, bf16[256,256]{1,0:T(8,128)(2,1)S(1)} %collective-permute-done.refs_2_, bf16[256,256]{1,0:T(8,128)(2,1)S(1)} %copy-done.17, ...), custom_call_target="tpu_custom_call" | custom-call | flops 6442450944 | bytes 4194304 | tf_op jit(solution)/shard_map/pallas_call | solution.py:161
  103.2 70.1 %all-gather.3.cloned.1.call-done.refs_5_ = bf16[4096,512]{1,0:T(8,128)(2,1)} async-done(((bf16[128,512]{1,0:T(8,128)(2,1)}), bf16[4096,512]{1,0:T(8,128)(2,1)}) %all-gather.3.cloned.1.call-update) | async-done | bytes 4194320 | tf_op jit(solution)/shard_map/all_gather | solution.py:365
  173.3 2.2 copy-done.14
  177.9 5.5 %shard_map.146 = (f32[1024,256]{1,0:T(8,128)S(1)}, f32[256,128]{1,0:T(8,128)S(1)}, bf16[1024,256]{1,0:T(8,128)(2,1)S(1)}, f32[256,128]{1,0:T(8,128)S(1)}) custom-call(s32[2]{0:T(128)S(1)} %pad_add_fusion.refs_0_, bf16[256,256]{1,0:T(8,128)(2,1)S(1)} %copy-done.16, bf16[256,256]{1,0:T(8,128)(2,1)S(1)} %collective-permute-done.refs_2_, ...), custom_call_target="tpu_custom_call" | custom-call | flops 6442450944 | bytes 4194304 | tf_op jit(solution)/shard_map/pallas_call | solution.py:161
  183.5 4.3 %collective-permute-start.2 = (bf16[1024,256]{1,0:T(8,128)(2,1)S(1)}, bf16[1024,256]{1,0:T(8,128)(2,1)S(1)}, u32[]{:S(2)}, u32[]{:S(2)}) collective-permute-start(bf16[1024,256]{1,0:T(8,128)(2,1)S(1)} %get-tuple-element.24), channel_id=1, source_target_pairs={{0,4},{4,0},{1,5},{5,1},{2,6},{6,2},{3,7},{7,3},{8,12},{12,8},{9,1... | collective-permute-start | bytes 1572872 | tf_op jit(solution)/shard_map/ppermute | solution.py:402
  189.5 3.7 project.1
  193.2 4.3 %all-to-all-start = ((bf16[4,64,2048]{2,1,0:T(8,128)(2,1)}), bf16[4,64,2048]{2,1,0:T(8,128)(2,1)}, u32[]{:S(2)}, u32[]{:S(2)}) async-start(bf16[4,64,2048]{2,1,0:T(8,128)(2,1)} %bitcast.5), calls=%async_computation | async-start | bytes 2097152 | tf_op jit(solution)/shard_map/all_to_all | solution.py:407
  201.7 10.6 %all-to-all-done.tiles = bf16[4,64,2048]{2,1,0:T(8,128)(2,1)} async-done(((bf16[4,64,2048]{2,1,0:T(8,128)(2,1)}), bf16[4,64,2048]{2,1,0:T(8,128)(2,1)}, u32[]{:S(2)}, u32[]{:S(2)}) %all-to-all-start) | async-done | bytes 1048608 | tf_op jit(solution)/shard_map/all_to_all | solution.py:407
  212.4 3.0 dispatch.1
  215.4 2.2 all_to_all.18
  217.6 20.1 %all-to-all-start.1 = ((bf16[64,4,2048]{2,1,0:T(4,128)(2,1)}), bf16[64,4,2048]{2,1,0:T(4,128)(2,1)}, u32[]{:S(2)}, u32[]{:S(2)}) async-start(bf16[64,4,2048]{2,1,0:T(4,128)(2,1)} %all_to_all.18), calls=%async_computation.1 | async-start | bytes 2097152 | tf_op jit(solution)/shard_map/all_to_all | solution.py:411
  241.4 9.5 %collective-permute-done.10.refs_10_ = bf16[1024,256]{1,0:T(8,128)(2,1)} collective-permute-done((bf16[1024,256]{1,0:T(8,128)(2,1)S(1)}, bf16[1024,256]{1,0:T(8,128)(2,1)}, u32[]{:S(2)}, u32[]{:S(2)}) %collective-permute-start.10) | collective-permute-done | bytes 524320 | tf_op jit(solution)/shard_map/ppermute | solution.py:375
  251.2 5.8 %collective-permute-done.6.refs_6_ = bf16[1024,256]{1,0:T(8,128)(2,1)S(1)} collective-permute-done((bf16[1024,256]{1,0:T(8,128)(2,1)S(1)}, bf16[1024,256]{1,0:T(8,128)(2,1)S(1)}, u32[]{:S(2)}, u32[]{:S(2)}) %collective-permute-start.6) | collective-permute-done | bytes 524320 | tf_op jit(solution)/shard_map/ppermute | solution.py:374
  258.6 3.6 collective-permute-done.9.refs_9_
  265.0 2.7 collective-permute-start.15
  267.7 22.9 %collective-permute-done.13.refs_13_ = bf16[1024,256]{1,0:T(8,128)(2,1)S(1)} collective-permute-done((bf16[1024,256]{1,0:T(8,128)(2,1)S(1)}, bf16[1024,256]{1,0:T(8,128)(2,1)S(1)}, u32[]{:S(2)}, u32[]{:S(2)}) %collective-permute-start.13) | collective-permute-done | bytes 524320 | tf_op jit(solution)/shard_map/ppermute | solution.py:376
  293.5 26.7 %collective-permute-done.14.refs_14_ = bf16[1024,256]{1,0:T(8,128)(2,1)} collective-permute-done((bf16[1024,256]{1,0:T(8,128)(2,1)}, bf16[1024,256]{1,0:T(8,128)(2,1)}, u32[]{:S(2)}, u32[]{:S(2)}) %collective-permute-start.14) | collective-permute-done | bytes 524320 | tf_op jit(solution)/shard_map/ppermute | solution.py:377
  325.6 5.3 %experts.1 = bf16[256,2048]{1,0:T(8,128)(2,1)S(1)} custom-call(bf16[256,2048]{1,0:T(8,128)(2,1)S(1)} %all_to_all.20.rows_in, bf16[2048,256]{1,0:T(8,128)(2,1)S(1)} %bitcast.17, bf16[1024,256]{1,0:T(8,128)(2,1)S(1)} %get-tuple-element.32.refs_1_, bf16[1024,256]{1,0:T(8,128)(2,1)S(1)} %get-tuple-element.31.refs_2_, bf16[256,2048]{1,0:T(8,128)(2,1)} %bitcast.10.refs_3_, ...), custom_call_target="tpu_custom_call" | custom-call | flops 3221225472 | bytes 12582912 | tf_op jit(solution)/shard_map/experts/pallas_call | solution.py:297
  332.2 16.8 %all-to-all-start.2 = ((bf16[64,4,2048]{2,1,0:T(4,128)(2,1)}), bf16[64,4,2048]{2,1,0:T(4,128)(2,1)S(1)}, u32[]{:S(2)}, u32[]{:S(2)}) async-start(bf16[64,4,2048]{2,1,0:T(4,128)(2,1)} %all_to_all.21), calls=%async_computation.2 | async-start | bytes 2097152 | tf_op jit(solution)/shard_map/all_to_all | solution.py:413
  349.7 27.5 %all-to-all-done.2 = bf16[64,4,2048]{2,1,0:T(4,128)(2,1)S(1)} async-done(((bf16[64,4,2048]{2,1,0:T(4,128)(2,1)}), bf16[64,4,2048]{2,1,0:T(4,128)(2,1)S(1)}, u32[]{:S(2)}, u32[]{:S(2)}) %all-to-all-start.2) | async-done | bytes 1048608 | tf_op jit(solution)/shard_map/all_to_all | solution.py:413
  378.2 2.6 collect.1
  (98 shorter events, 38.9 us)
Async XLA Ops:
  6.5 85.5 %all-gather.5.cloned.1.call-start = ((), (), s32[]{:S(2)}) async-start(), calls=%async_computation.4 | async-start | bytes 4325376 | tf_op jit(solution)/shard_map/all_gather | solution.py:365
  8.9 164.3 %all-gather.3.cloned.1.call-start = ((), (), s32[]{:S(2)}) async-start(), calls=%async_computation.3 | async-start | bytes 4325376 | tf_op jit(solution)/shard_map/all_gather | solution.py:365
  9.7 7.1 %collective-permute-start = (bf16[256,256]{1,0:T(8,128)(2,1)}, bf16[256,256]{1,0:T(8,128)(2,1)S(1)}, u32[]{:S(2)}, u32[]{:S(2)}) collective-permute-start(bf16[256,256]{1,0:T(8,128)(2,1)} %refs_1_.3), channel_id=1, source_target_pairs={{0,4},{4,0},{1,5},{5,1},{2,6},{6,2},{3,7},{7,3},{8,12},{12,8},{9,1... | collective-permute-start | bytes 393224 | tf_op jit(solution)/shard_map/ppermute | solution.py:367
  13.0 3.8 collective-permute-start.1
  96.1 77.2 %copy-start.16 = (bf16[256,256]{1,0:T(8,128)(2,1)S(1)}, bf16[256,256]{1,0:T(8,128)(2,1)}, u32[]{:S(2)}) copy-start(bf16[256,256]{1,0:T(8,128)(2,1)} %refs_1_.3) | copy-start | bytes 393220
  96.1 77.2 %copy-start.18 = (bf16[256,256]{1,0:T(8,128)(2,1)S(1)}, bf16[256,256]{1,0:T(8,128)(2,1)}, u32[]{:S(2)}) copy-start(bf16[256,256]{1,0:T(8,128)(2,1)} %refs_3_.3) | copy-start | bytes 393220
  183.5 6.0 %collective-permute-start.2 = (bf16[1024,256]{1,0:T(8,128)(2,1)S(1)}, bf16[1024,256]{1,0:T(8,128)(2,1)S(1)}, u32[]{:S(2)}, u32[]{:S(2)}) collective-permute-start(bf16[1024,256]{1,0:T(8,128)(2,1)S(1)} %get-tuple-element.24), channel_id=1, source_target_pairs={{0,4},{4,0},{1,5},{5,1},{2,6},{6,2},{3,7},{7,3},{8,12},{12,8},{9,1... | collective-permute-start | bytes 1572872 | tf_op jit(solution)/shard_map/ppermute | solution.py:402
  187.8 1.7 collective-permute-start.3
  193.2 19.2 %all-to-all-start = ((bf16[4,64,2048]{2,1,0:T(8,128)(2,1)}), bf16[4,64,2048]{2,1,0:T(8,128)(2,1)}, u32[]{:S(2)}, u32[]{:S(2)}) async-start(bf16[4,64,2048]{2,1,0:T(8,128)(2,1)} %bitcast.5), calls=%async_computation | async-start | bytes 2097152 | tf_op jit(solution)/shard_map/all_to_all | solution.py:407
  197.6 41.7 %collective-permute-start.5 = (bf16[1024,256]{1,0:T(8,128)(2,1)S(1)}, bf16[1024,256]{1,0:T(8,128)(2,1)S(1)}, u32[]{:S(2)}, u32[]{:S(2)}) collective-permute-start(bf16[1024,256]{1,0:T(8,128)(2,1)S(1)} %get-tuple-element.32.refs_1_), channel_id=1, source_target_pairs={{0,1},{1,2},{2,3},{3,0},{4,5},{5,6},{6,7},{7,4},{8,9},{9,10},{10,1... | collective-permute-start | bytes 1572872 | tf_op jit(solution)/shard_map/ppermute | solution.py:374
  199.1 66.0 %collective-permute-start.4 = (bf16[2048,256]{1,0:T(8,128)(2,1)S(1)}, bf16[2048,256]{1,0:T(8,128)(2,1)}, u32[]{:S(2)}, u32[]{:S(2)}) collective-permute-start(bf16[2048,256]{1,0:T(8,128)(2,1)S(1)} %bitcast.15), channel_id=1, source_target_pairs={{0,1},{1,2},{2,3},{3,0},{4,5},{5,6},{6,7},{7,4},{8,9},{9,10},{10,1... | collective-permute-start | bytes 3145736 | tf_op jit(solution)/shard_map/ppermute | solution.py:374
  200.3 64.8 %collective-permute-start.11 = (bf16[256,2048]{1,0:T(8,128)(2,1)}, bf16[256,2048]{1,0:T(8,128)(2,1)}, u32[]{:S(2)}, u32[]{:S(2)}) collective-permute-start(bf16[256,2048]{1,0:T(8,128)(2,1)} %bitcast.10.refs_3_), channel_id=1, source_target_pairs={{0,3},{1,0},{2,1},{3,2},{4,7},{5,4},{6,5},{7,6},{8,11},{9,8},{10,9... | collective-permute-start | bytes 3145736 | tf_op jit(solution)/shard_map/ppermute | solution.py:375
  217.6 74.5 %all-to-all-start.1 = ((bf16[64,4,2048]{2,1,0:T(4,128)(2,1)}), bf16[64,4,2048]{2,1,0:T(4,128)(2,1)}, u32[]{:S(2)}, u32[]{:S(2)}) async-start(bf16[64,4,2048]{2,1,0:T(4,128)(2,1)} %all_to_all.18), calls=%async_computation.1 | async-start | bytes 2097152 | tf_op jit(solution)/shard_map/all_to_all | solution.py:411
  237.8 13.1 %collective-permute-start.10 = (bf16[1024,256]{1,0:T(8,128)(2,1)S(1)}, bf16[1024,256]{1,0:T(8,128)(2,1)}, u32[]{:S(2)}, u32[]{:S(2)}) collective-permute-start(bf16[1024,256]{1,0:T(8,128)(2,1)S(1)} %get-tuple-element.31.refs_2_), channel_id=1, source_target_pairs={{0,3},{1,0},{2,1},{3,2},{4,7},{5,4},{6,5},{7,6},{8,11},{9,8},{10,9... | collective-permute-start | bytes 1572872 | tf_op jit(solution)/shard_map/ppermute | solution.py:375
  238.7 18.3 %collective-permute-start.6 = (bf16[1024,256]{1,0:T(8,128)(2,1)S(1)}, bf16[1024,256]{1,0:T(8,128)(2,1)S(1)}, u32[]{:S(2)}, u32[]{:S(2)}) collective-permute-start(bf16[1024,256]{1,0:T(8,128)(2,1)S(1)} %get-tuple-element.31.refs_2_), channel_id=1, source_target_pairs={{0,1},{1,2},{2,3},{3,0},{4,5},{5,6},{6,7},{7,4},{8,9},{9,10},{10,1... | collective-permute-start | bytes 1572872 | tf_op jit(solution)/shard_map/ppermute | solution.py:374
  239.3 22.8 %collective-permute-start.9 = (bf16[1024,256]{1,0:T(8,128)(2,1)S(1)}, bf16[1024,256]{1,0:T(8,128)(2,1)S(1)}, u32[]{:S(2)}, u32[]{:S(2)}) collective-permute-start(bf16[1024,256]{1,0:T(8,128)(2,1)S(1)} %get-tuple-element.32.refs_1_), channel_id=1, source_target_pairs={{0,3},{1,0},{2,1},{3,2},{4,7},{5,4},{6,5},{7,6},{8,11},{9,8},{10,9... | collective-permute-start | bytes 1572872 | tf_op jit(solution)/shard_map/ppermute | solution.py:375
  250.9 69.3 %collective-permute-start.7 = (bf16[256,2048]{1,0:T(8,128)(2,1)}, bf16[256,2048]{1,0:T(8,128)(2,1)}, u32[]{:S(2)}, u32[]{:S(2)}) collective-permute-start(bf16[256,2048]{1,0:T(8,128)(2,1)} %bitcast.10.refs_3_), channel_id=1, source_target_pairs={{0,1},{1,2},{2,3},{3,0},{4,5},{5,6},{6,7},{7,4},{8,9},{9,10},{10,1... | collective-permute-start | bytes 3145736 | tf_op jit(solution)/shard_map/ppermute | solution.py:374
  257.8 32.8 %collective-permute-start.13 = (bf16[1024,256]{1,0:T(8,128)(2,1)S(1)}, bf16[1024,256]{1,0:T(8,128)(2,1)S(1)}, u32[]{:S(2)}, u32[]{:S(2)}) collective-permute-start(bf16[1024,256]{1,0:T(8,128)(2,1)S(1)} %collective-permute-done.5.refs_5_), channel_id=1, source_target_pairs={{0,1},{1,2},{2,3},{3,0},{4,5},{5,6},{6,7},{7,4},{8,9},{9,10},{10,1... | collective-permute-start | bytes 1572872 | tf_op jit(solution)/shard_map/ppermute | solution.py:376
  262.9 57.3 %collective-permute-start.8 = (bf16[2048,256]{1,0:T(8,128)(2,1)S(1)}, bf16[2048,256]{1,0:T(8,128)(2,1)}, u32[]{:S(2)}, u32[]{:S(2)}) collective-permute-start(bf16[2048,256]{1,0:T(8,128)(2,1)S(1)} %bitcast.16), channel_id=1, source_target_pairs={{0,3},{1,0},{2,1},{3,2},{4,7},{5,4},{6,5},{7,6},{8,11},{9,8},{10,9... | collective-permute-start | bytes 3145736 | tf_op jit(solution)/shard_map/ppermute | solution.py:375
  265.0 55.2 %collective-permute-start.12 = (bf16[2048,256]{1,0:T(8,128)(2,1)}, bf16[2048,256]{1,0:T(8,128)(2,1)}, u32[]{:S(2)}, u32[]{:S(2)}) collective-permute-start(bf16[2048,256]{1,0:T(8,128)(2,1)} %collective-permute-done.4.refs_4_), channel_id=1, source_target_pairs={{0,1},{1,2},{2,3},{3,0},{4,5},{5,6},{6,7},{7,4},{8,9},{9,10},{10,1... | collective-permute-start | bytes 3145736 | tf_op jit(solution)/shard_map/ppermute | solution.py:376
  265.0 55.2 %collective-permute-start.15 = (bf16[256,2048]{1,0:T(8,128)(2,1)}, bf16[256,2048]{1,0:T(8,128)(2,1)}, u32[]{:S(2)}, u32[]{:S(2)}) collective-permute-start(bf16[256,2048]{1,0:T(8,128)(2,1)} %collective-permute-done.11.refs_11_), channel_id=1, source_target_pairs={{0,3},{1,0},{2,1},{3,2},{4,7},{5,4},{6,5},{7,6},{8,11},{9,8},{10,9... | collective-permute-start | bytes 3145736 | tf_op jit(solution)/shard_map/ppermute | solution.py:377
  291.4 28.8 %collective-permute-start.14 = (bf16[1024,256]{1,0:T(8,128)(2,1)}, bf16[1024,256]{1,0:T(8,128)(2,1)}, u32[]{:S(2)}, u32[]{:S(2)}) collective-permute-start(bf16[1024,256]{1,0:T(8,128)(2,1)} %collective-permute-done.10.refs_10_), channel_id=1, source_target_pairs={{0,3},{1,0},{2,1},{3,2},{4,7},{5,4},{6,5},{7,6},{8,11},{9,8},{10,9... | collective-permute-start | bytes 1572872 | tf_op jit(solution)/shard_map/ppermute | solution.py:377
  330.9 18.0 %copy-start.24 = (f32[64,2]{0,1:T(2,128)S(1)}, f32[64,2]{0,1:T(2,128)}, u32[]{:S(2)}) copy-start(f32[64,2]{0,1:T(2,128)} %param.26) | copy-start | bytes 1540
  332.2 44.9 %all-to-all-start.2 = ((bf16[64,4,2048]{2,1,0:T(4,128)(2,1)}), bf16[64,4,2048]{2,1,0:T(4,128)(2,1)S(1)}, u32[]{:S(2)}, u32[]{:S(2)}) async-start(bf16[64,4,2048]{2,1,0:T(4,128)(2,1)} %all_to_all.21), calls=%async_computation.2 | async-start | bytes 2097152 | tf_op jit(solution)/shard_map/all_to_all | solution.py:413
  (22 other events, 77.5 us)
Sparse Core Ops, SparseCore 0:
  9.9 82.1 all-gather.4
  94.6 78.5 all-gather.2
